TPU v7x, 512 devices: a whole 4x4x16 slice. The times are simulated.
512 devices in a mesh: sp: 128 (over z, x, core), tp: 4 (over y).
Axes of the slice: x: 4, y: 4, z: 16, core: 2. Of those that a mesh axis runs over, the one named last changes fastest.
Arguments:
- tokens: bfloat16 [49152, 2048], P('sp'), may hold values from -6 to 6
- doc_ids: int32 [49152], P('sp'), may hold values from 0 to 31, never falling along the last dimension, each value on 1 to 3072 neighbouring positions
- pre_gain: float32 [2, 2048], replicated, may hold values from 0.1 to 1.9
- value_proj: bfloat16 [2, 2048, 1024], P(None, 'sp', 'tp'), may hold values from -0.5 to 0.5
- gate_proj: bfloat16 [2, 2048, 1024], P(None, 'sp', 'tp'), may hold values from -0.5 to 0.5
- out_proj: bfloat16 [2, 1024, 2048], P(None, 'tp', 'sp'), may hold values from -0.1875 to 0.1875
- conv_taps: float32 [2, 31, 1024], P(None, None, 'tp'), may hold values from -2.2 to 2.2
- norm_gain: float32 [2, 1024], P(None, 'tp'), may hold values from 0.1 to 1.9
- norm_shift: float32 [2, 1024], P(None, 'tp'), may hold values from -3 to 3
Outputs:
- hidden: bfloat16 [49152, 2048], P('sp')
Inputs may be any that keep to these rules, and one draw needn't show every extreme that they name: `doc_ids`: document numbers never fall along the sequence; each document has 1 to 3072 positions.
All inputs are finite; a program needn't handle non-finite values.
Results may differ from a plain program's by a relative error of at most 0.017.
Values may be sent and summed in bfloat16 or wider, within the bound.
A program may use at most 64 MiB of HBM per device.

v0:
```python
import jax
import jax.numpy as jnp
from jax import lax
from jax.sharding import PartitionSpec as P

epsilon = 1e-06


def rows_first(arrays, axis, dims):
    turned = [jnp.moveaxis(a, dim, 0) for a, dim in zip(arrays, dims)]
    both = jnp.concatenate([t.reshape(len(t), -1) for t in turned], axis=1)
    out, at, outs = (lax.all_gather(both, axis, axis=0, tiled=True), 0, [])
    for t, dim in zip(turned, dims):
        slab = out[:, at : at + t[0].size].reshape(-1, *t.shape[1:])
        outs.append(jnp.moveaxis(slab, 0, dim))
        at += t[0].size
    return tuple(outs)


def passed_along(value, axis, steps):
    count = lax.axis_size(axis)
    first, last = (max(0, -steps), min(count, count - steps))
    return lax.ppermute(value, axis, [(source, source + steps) for source in range(first, last)])


def sent_to_all(value, axis):
    copies = jnp.broadcast_to(value, (lax.axis_size(axis), *value.shape))
    return lax.all_to_all(copies, axis, split_axis=0, concat_axis=0, tiled=True)


def taken_together(value, axis):
    everything = sent_to_all(value, axis)
    return jnp.sum(everything, axis=0)


def together(arrays, axis):
    ravelled, at, outs = (jnp.concatenate([a.reshape(-1) for a in arrays]), 0, [])
    total = taken_together(ravelled, axis)
    for a in arrays:
        outs.append(total[at : at + a.size].reshape(a.shape))
        at += a.size
    return tuple(outs)


def cut_along(value, dim, length):
    before, after = (value.shape[:dim], value.shape[dim + 1 :])
    return jnp.moveaxis(value.reshape(*before, length, -1, *after), dim, 0)


def summed_on_arrival(value, axis, dim):
    pieces = cut_along(value, dim, lax.axis_size(axis))
    arrived = lax.all_to_all(pieces, axis, split_axis=0, concat_axis=0, tiled=True)
    return arrived.astype(jnp.float32).sum(axis=0)


def in_order(pieces, dim):
    lengths = list(pieces.shape[1:])
    lengths[dim] *= pieces.shape[0]
    return jnp.moveaxis(pieces, 0, dim).reshape(lengths)


def collect(value, axis, dim):
    return in_order(sent_to_all(value, axis), dim)


def on_device(
    tokens, doc_ids, pre_gain, value_proj, gate_proj, out_proj, conv_taps, norm_gain, norm_shift
):
    layer_count = value_proj.shape[0]
    tap_count = conv_taps.shape[1]
    reach_rows = tap_count - 1
    row_count = tokens.shape[0]
    block_width = conv_taps.shape[2]
    channels = block_width * lax.axis_size("tp")
    hidden = tokens
    full_value, full_gate, full_out = rows_first((value_proj, gate_proj, out_proj), "sp", (1, 1, 2))
    for layer_index in range(layer_count):
        wide_state = hidden.astype(jnp.float32)
        scale = lax.rsqrt(jnp.mean(wide_state * wide_state, axis=-1, keepdims=True) + epsilon)
        normed = (wide_state * scale * pre_gain[layer_index]).astype(jnp.bfloat16)
        value_acc = jnp.dot(normed, full_value[layer_index], preferred_element_type=jnp.float32)
        gate_acc = jnp.dot(normed, full_gate[layer_index], preferred_element_type=jnp.float32)
        value_half = value_acc.astype(jnp.bfloat16)
        gate_half = gate_acc.astype(jnp.bfloat16)
        gated_rows = (
            value_half.astype(jnp.float32) * jax.nn.sigmoid(gate_half.astype(jnp.float32))
        ).astype(jnp.bfloat16)
        prev_rows, prev_docs = passed_along(
            (gated_rows[row_count - reach_rows :], doc_ids[row_count - reach_rows :]), "sp", 1
        )
        padded = jnp.concatenate([prev_rows, gated_rows]).astype(jnp.float32)
        padded_docs = jnp.concatenate([prev_docs, doc_ids])
        conv_out = jnp.zeros((row_count, block_width), jnp.float32)
        for offset in range(tap_count):
            first_row = reach_rows - offset
            same_doc = (padded_docs[first_row : first_row + row_count] == doc_ids)[:, None]
            term = (
                conv_taps[layer_index, offset][None, :] * padded[first_row : first_row + row_count]
            )
            conv_out = conv_out + jnp.where(same_doc, term, jnp.float32(0.0))
        row_sums, square_sums = together(
            (jnp.sum(conv_out, axis=1), jnp.sum(conv_out * conv_out, axis=1)), "tp"
        )
        row_mean = (row_sums / channels)[:, None]
        row_var = (square_sums / channels)[:, None] - row_mean * row_mean
        normalized = (
            norm_gain[layer_index] * (conv_out - row_mean) * lax.rsqrt(row_var + epsilon)
            + norm_shift[layer_index]
        )
        activated = jax.nn.silu(normalized).astype(jnp.bfloat16)
        partial_value = jnp.dot(
            activated, full_out[layer_index], preferred_element_type=jnp.float32
        )
        summed = summed_on_arrival(partial_value.astype(jnp.bfloat16), "tp", 1)
        branch = summed.astype(jnp.bfloat16)
        piece_width = summed.shape[1]
        own_cols = lax.dynamic_slice_in_dim(
            hidden, lax.axis_index("tp") * piece_width, piece_width, 1
        )
        updated = (own_cols.astype(jnp.float32) + branch.astype(jnp.float32)).astype(jnp.bfloat16)
        hidden = collect(updated, "tp", 1)
    return hidden


def solution(mesh):
    return jax.shard_map(
        on_device,
        mesh=mesh,
        in_specs=(
            P("sp", None),
            P("sp"),
            P(),
            P(None, "sp", "tp"),
            P(None, "sp", "tp"),
            P(None, "tp", "sp"),
            P(None, None, "tp"),
            P(None, "tp"),
            P(None, "tp"),
        ),
        out_specs=P("sp", None),
        check_vma=False,
    )
```

profile of v0, /device:TPU:36, one launch (start us, length us, event | category | flops | bytes accessed | tf_op | source)
XLA Modules:
  0.0 315.1 jit_solution(1334254646113636902)
XLA Ops:
  6.5 0.7 copy.87
  7.3 0.7 copy.88
  8.0 0.7 copy.86
  9.3 0.8 slice.568
  10.1 1.9 collective-permute-start.1
  12.0 1.8 fusion
  13.8 0.8 fusion.164
  14.6 0.9 fusion.163
  15.5 0.9 fusion.162
  16.3 0.8 slice_reduce_fusion
  17.2 0.8 fusion.165
  17.9 0.8 pad_add_fusion
  18.7 0.8 slice_compare_fusion.29
  19.5 137.9 %all-gather.2.cloned.1.call-done = bf16[2048,1536]{1,0:T(8,128)(2,1)} async-done(((bf16[16,1536]{1,0:T(8,128)(2,1)}), bf16[2048,1536]{1,0:T(8,128)(2,1)}) %all-gather.2.cloned.1.call-update) | async-done | bytes 6291472 | tf_op jit(solution)/shard_map/all_gather | solution.py:12
  157.4 3.4 %fusion.160 = (bf16[2048,512]{1,0:T(8,128)(2,1)S(1)}, bf16[2048,512]{1,0:T(8,128)(2,1)S(1)}, bf16[2048,512]{1,0:T(8,128)(2,1)S(1)}) fusion(bf16[2048,1536]{1,0:T(8,128)(2,1)} %all-gather.2.cloned.1.call-done), kind=kLoop, calls=%fused_computation.288 | loop fusion | bytes 12582912 | tf_op jit(solution)/shard_map/slice | solution.py:14
  161.1 1.1 copy-done
  162.3 1.3 copy-done.2
  163.6 0.6 fusion.21
  164.2 0.6 fusion.20
  164.9 2.1 collective-permute-start
  167.1 2.8 collective-permute-done
  170.0 3.3 %fusion.157 = (f32[384]{0:T(512)S(1)}, f32[384]{0:T(512)S(1)}, f32[384,256]{1,0:T(8,128)S(1)}) fusion(f32[414,256]{1,0:T(8,128)S(1)} %maximum_convert_fusion, f32[256]{0:T(256)S(1)} %bitcast.193, pred[384]{0:T(512)(128)(4,1)S(1)} %get-tuple-element.110, f32[256]{0:T(256)S(1)} %bitcast.194, pred[384]{0:T(512)(128)(4,1)S(1)} %get-tuple-element.111, ...), kind=kLoop, calls=%fused_computation.287 | loop fusion | flops 9239808 | bytes 12629248 | tf_op jit(solution)/shard_map/reduce_sum | solution.py:102
  174.0 4.2 %all-to-all-start = ((f32[4,1,768]{2,1,0:T(1,128)}), f32[4,1,768]{2,1,0:T(1,128)S(1)}, u32[]{:S(2)}, u32[]{:S(2)}) async-start(f32[4,1,768]{2,1,0:T(1,128)} %broadcast_in_dim.423), calls=%async_computation | async-start | bytes 24576 | tf_op jit(solution)/shard_map/all_to_all | solution.py:28
  178.2 2.5 copy.74
  180.6 2.9 all-to-all-done
  183.5 1.9 convolution_convert_fusion.1
  185.4 1.3 copy.96
  186.7 3.6 %all-to-all-start.1 = ((bf16[4,384,512]{2,1,0:T(8,128)(2,1)}), bf16[4,384,512]{2,1,0:T(8,128)(2,1)S(1)}, u32[]{:S(2)}, u32[]{:S(2)}) async-start(bf16[4,384,512]{2,1,0:T(8,128)(2,1)} %bitcast.135), calls=%async_computation.1 | async-start | bytes 3145728 | tf_op jit(solution)/shard_map/all_to_all | solution.py:52
  190.3 18.3 %all-to-all-done.1 = bf16[4,384,512]{2,1,0:T(8,128)(2,1)S(1)} async-done(((bf16[4,384,512]{2,1,0:T(8,128)(2,1)}), bf16[4,384,512]{2,1,0:T(8,128)(2,1)S(1)}, u32[]{:S(2)}, u32[]{:S(2)}) %all-to-all-start.1) | async-done | bytes 1572896 | tf_op jit(solution)/shard_map/all_to_all | solution.py:52
  209.0 1.1 add_convert_fusion.1
  210.1 1.3 broadcast_in_dim.424
  211.4 3.6 %all-to-all-start.2 = ((bf16[4,384,512]{2,1,0:T(8,128)(2,1)}), bf16[4,384,512]{2,1,0:T(8,128)(2,1)S(1)}, u32[]{:S(2)}, u32[]{:S(2)}) async-start(bf16[4,384,512]{2,1,0:T(8,128)(2,1)} %broadcast_in_dim.424), calls=%async_computation.2 | async-start | bytes 3145728 | tf_op jit(solution)/shard_map/all_to_all | solution.py:28
  215.0 17.5 %all-to-all-done.2 = bf16[4,384,512]{2,1,0:T(8,128)(2,1)S(1)} async-done(((bf16[4,384,512]{2,1,0:T(8,128)(2,1)}), bf16[4,384,512]{2,1,0:T(8,128)(2,1)S(1)}, u32[]{:S(2)}, u32[]{:S(2)}) %all-to-all-start.2) | async-done | bytes 1572896 | tf_op jit(solution)/shard_map/all_to_all | solution.py:28
  232.5 0.9 copy.68
  234.2 0.7 copy-done.1
  235.9 0.7 fusion.12
  236.6 1.9 collective-permute-start.2
  238.5 0.9 fusion.161
  239.4 2.2 collective-permute-done.2
  241.7 3.3 %fusion.156 = (f32[384]{0:T(512)S(1)}, f32[384]{0:T(512)S(1)}, f32[384,256]{1,0:T(8,128)S(1)}) fusion(f32[414,256]{1,0:T(8,128)S(1)} %maximum_convert_fusion.1, f32[256]{0:T(256)S(1)} %bitcast.159, pred[384]{0:T(512)(128)(4,1)S(1)} %get-tuple-element.110, f32[256]{0:T(256)S(1)} %bitcast.160, pred[384]{0:T(512)(128)(4,1)S(1)} %get-tuple-element.111, ...), kind=kLoop, calls=%fused_computation.286 | loop fusion | flops 9239808 | bytes 12629248 | tf_op jit(solution)/shard_map/reduce_sum | solution.py:102
  245.1 7.7 %all_to_all.32 = f32[4,1,768]{2,1,0:T(1,128)S(1)} all-to-all(f32[4,1,768]{2,1,0:T(1,128)S(1)} %broadcast_in_dim.425), channel_id=1, replica_groups=mesh['sp'=128,'tp'=4] {'tp'}, dimensions={0} | all-to-all | bytes 24576 | tf_op jit(solution)/shard_map/all_to_all | solution.py:28
  252.8 1.9 convolution_convert_fusion
  254.7 1.3 copy.95
  255.9 3.6 %all-to-all-start.4 = ((bf16[4,384,512]{2,1,0:T(8,128)(2,1)}), bf16[4,384,512]{2,1,0:T(8,128)(2,1)S(1)}, u32[]{:S(2)}, u32[]{:S(2)}) async-start(bf16[4,384,512]{2,1,0:T(8,128)(2,1)} %bitcast.139), calls=%async_computation.4 | async-start | bytes 3145728 | tf_op jit(solution)/shard_map/all_to_all | solution.py:52
  259.8 21.7 %all-to-all-done.4 = bf16[4,384,512]{2,1,0:T(8,128)(2,1)S(1)} async-done(((bf16[4,384,512]{2,1,0:T(8,128)(2,1)}), bf16[4,384,512]{2,1,0:T(8,128)(2,1)S(1)}, u32[]{:S(2)}, u32[]{:S(2)}) %all-to-all-start.4) | async-done | bytes 1572896 | tf_op jit(solution)/shard_map/all_to_all | solution.py:52
  282.2 23.6 %all_to_all.33 = bf16[4,384,512]{2,1,0:T(8,128)(2,1)S(1)} all-to-all(bf16[4,384,512]{2,1,0:T(8,128)(2,1)S(1)} %broadcast_in_dim.426), channel_id=1, replica_groups=mesh['sp'=128,'tp'=4] {'tp'}, dimensions={0} | all-to-all | bytes 3145728 | tf_op jit(solution)/shard_map/all_to_all | solution.py:28
  305.8 0.9 copy.72
  306.6 1.6 copy.73
  (43 shorter events, 5.0 us)
Async XLA Ops:
  6.5 150.9 %all-gather.2.cloned.1.call-start = ((), (), s32[]{:S(2)}) async-start(), calls=%async_computation.6 | async-start | bytes 6340608 | tf_op jit(solution)/shard_map/all_gather | solution.py:12
  10.1 7.8 %collective-permute-start.1 = (s32[30]{0:T(128)S(1)}, s32[30]{0:T(128)S(1)}, u32[]{:S(2)}, u32[]{:S(2)}) collective-permute-start(s32[30]{0:T(128)S(1)} %slice.568), channel_id=1, source_target_pairs={{0,4},{4,8},{8,12},{12,16},{16,20},{20,24},{24,28},{28,32},{32,36}... | collective-permute-start | bytes 368 | tf_op jit(solution)/shard_map/ppermute | solution.py:23
  161.0 1.3 copy-start
  161.0 2.6 copy-start.2
  161.1 3.1 copy-start.3
  164.2 2.8 copy-start.5
  164.9 5.1 %collective-permute-start = (bf16[30,256]{1,0:T(8,128)(2,1)S(1)}, bf16[30,256]{1,0:T(8,128)(2,1)S(1)}, u32[]{:S(2)}, u32[]{:S(2)}) collective-permute-start(bf16[30,256]{1,0:T(8,128)(2,1)S(1)} %slice.739), channel_id=1, source_target_pairs={{0,4},{4,8},{8,12},{12,16},{16,20},{20,24},{24,28},{28,32},{32,36}... | collective-permute-start | bytes 46088 | tf_op jit(solution)/shard_map/ppermute | solution.py:23
  170.0 8.2 %copy-start.6 = (f32[2,256]{1,0:T(2,128)S(1)}, f32[2,256]{1,0:T(2,128)}, u32[]{:S(2)}) copy-start(f32[2,256]{1,0:T(2,128)} %param.17) | copy-start | bytes 6148
  174.0 9.6 %all-to-all-start = ((f32[4,1,768]{2,1,0:T(1,128)}), f32[4,1,768]{2,1,0:T(1,128)S(1)}, u32[]{:S(2)}, u32[]{:S(2)}) async-start(f32[4,1,768]{2,1,0:T(1,128)} %broadcast_in_dim.423), calls=%async_computation | async-start | bytes 24576 | tf_op jit(solution)/shard_map/all_to_all | solution.py:28
  186.7 21.9 %all-to-all-start.1 = ((bf16[4,384,512]{2,1,0:T(8,128)(2,1)}), bf16[4,384,512]{2,1,0:T(8,128)(2,1)S(1)}, u32[]{:S(2)}, u32[]{:S(2)}) async-start(bf16[4,384,512]{2,1,0:T(8,128)(2,1)} %bitcast.135), calls=%async_computation.1 | async-start | bytes 3145728 | tf_op jit(solution)/shard_map/all_to_all | solution.py:52
  211.4 21.0 %all-to-all-start.2 = ((bf16[4,384,512]{2,1,0:T(8,128)(2,1)}), bf16[4,384,512]{2,1,0:T(8,128)(2,1)S(1)}, u32[]{:S(2)}, u32[]{:S(2)}) async-start(bf16[4,384,512]{2,1,0:T(8,128)(2,1)} %broadcast_in_dim.424), calls=%async_computation.2 | async-start | bytes 3145728 | tf_op jit(solution)/shard_map/all_to_all | solution.py:28
  233.3 1.6 copy-start.1
  234.2 1.7 copy-start.4
  236.6 5.1 %collective-permute-start.2 = (bf16[30,256]{1,0:T(8,128)(2,1)S(1)}, bf16[30,256]{1,0:T(8,128)(2,1)S(1)}, u32[]{:S(2)}, u32[]{:S(2)}) collective-permute-start(bf16[30,256]{1,0:T(8,128)(2,1)S(1)} %slice.775), channel_id=1, source_target_pairs={{0,4},{4,8},{8,12},{12,16},{16,20},{20,24},{24,28},{28,32},{32,36}... | collective-permute-start | bytes 46088 | tf_op jit(solution)/shard_map/ppermute | solution.py:23
  255.9 25.5 %all-to-all-start.4 = ((bf16[4,384,512]{2,1,0:T(8,128)(2,1)}), bf16[4,384,512]{2,1,0:T(8,128)(2,1)S(1)}, u32[]{:S(2)}, u32[]{:S(2)}) async-start(bf16[4,384,512]{2,1,0:T(8,128)(2,1)} %bitcast.139), calls=%async_computation.4 | async-start | bytes 3145728 | tf_op jit(solution)/shard_map/all_to_all | solution.py:52
Sparse Core Ops, SparseCore 0:
  10.5 146.8 all-gather.1
where the time goes:
time: 316 us; the launch traced here: 315 us
  waiting for transfers between devices  203 us (64%)
  blocking collectives  31.3 us (10%)
  local copies, waits for them, and re-layouts  25.7 us (8%)
  starting transfers between devices  20.9 us (7%)
  between operations  13.8 us (4%)
  other arithmetic  13.7 us (4%)
  matrix products  6.31 us (2%)
    all_gather x1, waiting for transfers between devices, rows_first(): out, at, outs = (lax.all_gather(both, axis, axis=0, tiled=True), 0, [])  138 us
    all_to_all x2, waiting for transfers between devices, summed_on_arrival(): lax.all_to_all(pieces, axis, split_axis=0, concat_axis=0, tiled=True)  40 us
    all_to_all x2, blocking collectives, sent_to_all(): return lax.all_to_all(copies, axis, split_axis=0, concat_axis=0, tiled=True)  31.3 us
    all_to_all x2, waiting for transfers between devices, sent_to_all(): return lax.all_to_all(copies, axis, split_axis=0, concat_axis=0, tiled=True)  20.3 us
    all_to_all x2, starting transfers between devices, sent_to_all(): return lax.all_to_all(copies, axis, split_axis=0, concat_axis=0, tiled=True)  7.77 us
    all_to_all x2, starting transfers between devices, summed_on_arrival(): lax.all_to_all(pieces, axis, split_axis=0, concat_axis=0, tiled=True)  7.13 us
    reduce_sum x2, other arithmetic, on_device(): jnp.sum(conv_out, axis=1)  6.63 us
  transfers between devices with their start and end apart: 8, of which 7 were waited for; matrix products, arithmetic and copies ran while one was open for 4% of the time, Pallas kernels for 0%

commit v1 on v0

--- a/solution.py
+++ b/solution.py
@@ -9,7 +9,13 @@
 def rows_first(arrays, axis, dims):
     turned = [jnp.moveaxis(a, dim, 0) for a, dim in zip(arrays, dims)]
     both = jnp.concatenate([t.reshape(len(t), -1) for t in turned], axis=1)
-    out, at, outs = (lax.all_gather(both, axis, axis=0, tiled=True), 0, [])
+    out, at, outs = (
+        jnp.concatenate(
+            lax.all_to_all(jnp.stack([both] * lax.axis_size(axis)), axis, 0, 0), axis=0
+        ),
+        0,
+        [],
+    )
     for t, dim in zip(turned, dims):
         slab = out[:, at : at + t[0].size].reshape(-1, *t.shape[1:])
         outs.append(jnp.moveaxis(slab, 0, dim))

time: 316 us -> 462 us (1.46)
  the two profiles are of different devices: /device:TPU:36 before, /device:TPU:6 now
where the time goes in v1:
time: 462 us; the launch traced here: 461 us
  waiting for transfers between devices  341 us (74%)
  starting transfers between devices  41.1 us (9%)
  local copies, waits for them, and re-layouts  31.8 us (7%)
  blocking collectives  27.3 us (6%)
  other arithmetic  10.4 us (2%)
  matrix products  8.18 us (2%)
    all_to_all x1, waiting for transfers between devices, rows_first(): lax.all_to_all(jnp.stack([both] * lax.axis_size(axis)), axis, 0, 0)  269 us
    all_to_all x2, waiting for transfers between devices, summed_on_arrival(): lax.all_to_all(pieces, axis, split_axis=0, concat_axis=0, tiled=True)  39.5 us
    all_to_all x2, blocking collectives, sent_to_all(): return lax.all_to_all(copies, axis, split_axis=0, concat_axis=0, tiled=True)  27.3 us
    all_to_all x2, waiting for transfers between devices, sent_to_all(): return lax.all_to_all(copies, axis, split_axis=0, concat_axis=0, tiled=True)  23.8 us
    all_to_all x1, starting transfers between devices, rows_first(): lax.all_to_all(jnp.stack([both] * lax.axis_size(axis)), axis, 0, 0)  19.9 us
    slice x3, local copies, waits for them, and re-layouts, rows_first(): slab = out[:, at:at + t[0].size].reshape(-1, *t.shape[1:])  13.3 us
  transfers between devices with their start and end apart: 8, of which 8 were waited for; matrix products, arithmetic and copies ran while one was open for 1% of the time, Pallas kernels for 0%

profile of v1, /device:TPU:6, one launch (start us, length us, event | category | flops | bytes accessed | tf_op | source)
XLA Modules:
  0.0 460.6 jit_solution(16711752827725216015)
XLA Ops:
  0.0 0.7 copy.112
  0.7 0.7 copy.113
  1.4 0.7 copy.114
  2.2 3.4 stack.2
  5.6 19.9 %all-to-all-start = ((bf16[128,16,1536]{2,1,0:T(8,128)(2,1)}), bf16[128,16,1536]{2,1,0:T(8,128)(2,1)}, u32[]{:S(2)}, u32[]{:S(2)}) async-start(bf16[128,16,1536]{2,1,0:T(8,128)(2,1)} %stack.2), calls=%async_computation | async-start | bytes 12582912 | tf_op jit(solution)/shard_map/all_to_all | solution.py:14
  25.6 2.0 collective-permute-start.1
  28.2 2.7 collective-permute-done.1
  31.1 269.4 %all-to-all-done = bf16[128,16,1536]{2,1,0:T(8,128)(2,1)} async-done(((bf16[128,16,1536]{2,1,0:T(8,128)(2,1)}), bf16[128,16,1536]{2,1,0:T(8,128)(2,1)}, u32[]{:S(2)}, u32[]{:S(2)}) %all-to-all-start) | async-done | bytes 6291488 | tf_op jit(solution)/shard_map/all_to_all | solution.py:14
  300.5 5.4 %fusion.160 = (bf16[2048,512]{1,0:T(8,128)(2,1)}, bf16[2048,512]{1,0:T(8,128)(2,1)S(1)}, bf16[2048,512]{1,0:T(8,128)(2,1)}) fusion(bf16[2048,1536]{1,0:T(8,128)(2,1)} %bitcast.6), kind=kLoop, calls=%fused_computation.286 | loop fusion | bytes 12582912 | tf_op jit(solution)/shard_map/slice | solution.py:20
  306.0 3.9 copy.87
  309.9 4.0 copy.89
  313.9 2.5 fusion.21
  316.7 0.7 fusion.20
  317.4 1.9 collective-permute-start
  319.4 3.0 collective-permute-done
  322.5 3.3 fusion.157
  325.9 0.6 broadcast_in_dim.423
  326.5 4.5 all-to-all-start.1
  331.0 2.5 copy.102
  333.4 2.8 all-to-all-done.1
  336.3 1.9 convolution_convert_fusion.1
  338.2 1.3 copy.118
  339.5 3.6 all-to-all-start.2
  343.0 21.8 %all-to-all-done.2 = bf16[4,384,512]{2,1,0:T(8,128)(2,1)S(1)} async-done(((bf16[4,384,512]{2,1,0:T(8,128)(2,1)}), bf16[4,384,512]{2,1,0:T(8,128)(2,1)S(1)}, u32[]{:S(2)}, u32[]{:S(2)}) %all-to-all-start.2) | async-done | bytes 1572896 | tf_op jit(solution)/shard_map/all_to_all | solution.py:58
  364.8 0.4 reduce_sum.100
  365.3 1.1 add_convert_fusion.1
  366.4 1.3 broadcast_in_dim.424
  367.7 3.6 all-to-all-start.3
  371.2 20.9 %all-to-all-done.3 = bf16[4,384,512]{2,1,0:T(8,128)(2,1)S(1)} async-done(((bf16[4,384,512]{2,1,0:T(8,128)(2,1)}), bf16[4,384,512]{2,1,0:T(8,128)(2,1)S(1)}, u32[]{:S(2)}, u32[]{:S(2)}) %all-to-all-start.3) | async-done | bytes 1572896 | tf_op jit(solution)/shard_map/all_to_all | solution.py:34
  392.2 0.9 copy.94
  393.1 0.4 fusion.3
  393.5 0.4 fusion.5
  393.9 0.7 copy-done.2
  394.6 0.6 fusion.13
  395.3 1.0 copy-done.4
  396.2 0.7 fusion.12
  396.9 2.1 collective-permute-start.2
  399.1 2.9 collective-permute-done.2
  402.0 3.3 fusion.156
  405.4 7.7 %all_to_all.37 = f32[4,1,768]{2,1,0:T(1,128)S(1)} all-to-all(f32[4,1,768]{2,1,0:T(1,128)S(1)} %broadcast_in_dim.425), channel_id=1, replica_groups=mesh['sp'=128,'tp'=4] {'tp'}, dimensions={0} | all-to-all | bytes 24576 | tf_op jit(solution)/shard_map/all_to_all | solution.py:34
  413.1 1.9 convolution_convert_fusion
  415.0 1.3 copy.117
  416.3 3.6 all-to-all-start.5
  420.1 17.8 %all-to-all-done.5 = bf16[4,384,512]{2,1,0:T(8,128)(2,1)S(1)} async-done(((bf16[4,384,512]{2,1,0:T(8,128)(2,1)}), bf16[4,384,512]{2,1,0:T(8,128)(2,1)S(1)}, u32[]{:S(2)}, u32[]{:S(2)}) %all-to-all-start.5) | async-done | bytes 1572896 | tf_op jit(solution)/shard_map/all_to_all | solution.py:58
  437.8 0.4 reduce_sum.105
  438.5 19.6 %all_to_all.38 = bf16[4,384,512]{2,1,0:T(8,128)(2,1)S(1)} all-to-all(bf16[4,384,512]{2,1,0:T(8,128)(2,1)S(1)} %broadcast_in_dim.426), channel_id=1, replica_groups=mesh['sp'=128,'tp'=4] {'tp'}, dimensions={0} | all-to-all | bytes 3145728 | tf_op jit(solution)/shard_map/all_to_all | solution.py:34
  458.1 0.9 copy.100
  459.0 1.6 copy.101
  (49 shorter events, 1.9 us)
Async XLA Ops:
  5.6 19.9 %copy-start.6 = (s32[384]{0:T(512)S(1)}, s32[384]{0:T(512)}, u32[]{:S(2)}) copy-start(s32[384]{0:T(512)} %param.10) | copy-start | bytes 4612
  5.6 22.0 %copy-start = (bf16[384,2048]{1,0:T(8,128)(2,1)S(1)}, bf16[384,2048]{1,0:T(8,128)(2,1)}, u32[]{:S(2)}) copy-start(bf16[384,2048]{1,0:T(8,128)(2,1)} %param.9) | copy-start | bytes 4718596
  5.6 22.5 %copy-start.5 = (f32[2,31,256]{2,0,1:T(2,128)S(1)}, f32[2,31,256]{2,0,1:T(2,128)}, u32[]{:S(2)}) copy-start(f32[2,31,256]{2,0,1:T(2,128)} %param.15) | copy-start | bytes 190468
  5.6 22.5 %copy-start.7 = (f32[2,2048]{1,0:T(2,128)S(1)}, f32[2,2048]{1,0:T(2,128)}, u32[]{:S(2)}) copy-start(f32[2,2048]{1,0:T(2,128)} %param.11) | copy-start | bytes 49156
  5.6 22.6 %copy-start.8 = (f32[2,256]{1,0:T(2,128)S(1)}, f32[2,256]{1,0:T(2,128)}, u32[]{:S(2)}) copy-start(f32[2,256]{1,0:T(2,128)} %param.16) | copy-start | bytes 6148
  5.6 294.9 %all-to-all-start = ((bf16[128,16,1536]{2,1,0:T(8,128)(2,1)}), bf16[128,16,1536]{2,1,0:T(8,128)(2,1)}, u32[]{:S(2)}, u32[]{:S(2)}) async-start(bf16[128,16,1536]{2,1,0:T(8,128)(2,1)} %stack.2), calls=%async_computation | async-start | bytes 12582912 | tf_op jit(solution)/shard_map/all_to_all | solution.py:14
  25.6 5.3 %collective-permute-start.1 = (s32[30]{0:T(128)S(1)}, s32[30]{0:T(128)S(1)}, u32[]{:S(2)}, u32[]{:S(2)}) collective-permute-start(s32[30]{0:T(128)S(1)} %slice.568), channel_id=1, source_target_pairs={{0,4},{4,8},{8,12},{12,16},{16,20},{20,24},{24,28},{28,32},{32,36}... | collective-permute-start | bytes 368 | tf_op jit(solution)/shard_map/ppermute | solution.py:29
  313.9 2.5 copy-start.1
  313.9 2.9 copy-start.3
  317.4 5.1 %collective-permute-start = (bf16[30,256]{1,0:T(8,128)(2,1)S(1)}, bf16[30,256]{1,0:T(8,128)(2,1)S(1)}, u32[]{:S(2)}, u32[]{:S(2)}) collective-permute-start(bf16[30,256]{1,0:T(8,128)(2,1)S(1)} %slice.739), channel_id=1, source_target_pairs={{0,4},{4,8},{8,12},{12,16},{16,20},{20,24},{24,28},{28,32},{32,36}... | collective-permute-start | bytes 46088 | tf_op jit(solution)/shard_map/ppermute | solution.py:29
  322.5 8.4 %copy-start.9 = (f32[2,256]{1,0:T(2,128)S(1)}, f32[2,256]{1,0:T(2,128)}, u32[]{:S(2)}) copy-start(f32[2,256]{1,0:T(2,128)} %param.17) | copy-start | bytes 6148
  326.5 9.8 %all-to-all-start.1 = ((f32[4,1,768]{2,1,0:T(1,128)}), f32[4,1,768]{2,1,0:T(1,128)S(1)}, u32[]{:S(2)}, u32[]{:S(2)}) async-start(f32[4,1,768]{2,1,0:T(1,128)} %broadcast_in_dim.423), calls=%async_computation.1 | async-start | bytes 24576 | tf_op jit(solution)/shard_map/all_to_all | solution.py:34
  339.5 25.4 %all-to-all-start.2 = ((bf16[4,384,512]{2,1,0:T(8,128)(2,1)}), bf16[4,384,512]{2,1,0:T(8,128)(2,1)S(1)}, u32[]{:S(2)}, u32[]{:S(2)}) async-start(bf16[4,384,512]{2,1,0:T(8,128)(2,1)} %bitcast.132), calls=%async_computation.2 | async-start | bytes 3145728 | tf_op jit(solution)/shard_map/all_to_all | solution.py:58
  367.7 24.5 %all-to-all-start.3 = ((bf16[4,384,512]{2,1,0:T(8,128)(2,1)}), bf16[4,384,512]{2,1,0:T(8,128)(2,1)S(1)}, u32[]{:S(2)}, u32[]{:S(2)}) async-start(bf16[4,384,512]{2,1,0:T(8,128)(2,1)} %broadcast_in_dim.424), calls=%async_computation.3 | async-start | bytes 3145728 | tf_op jit(solution)/shard_map/all_to_all | solution.py:34
  393.1 1.6 copy-start.2
  394.6 1.6 copy-start.4
  396.9 5.1 %collective-permute-start.2 = (bf16[30,256]{1,0:T(8,128)(2,1)S(1)}, bf16[30,256]{1,0:T(8,128)(2,1)S(1)}, u32[]{:S(2)}, u32[]{:S(2)}) collective-permute-start(bf16[30,256]{1,0:T(8,128)(2,1)S(1)} %slice.775), channel_id=1, source_target_pairs={{0,4},{4,8},{8,12},{12,16},{16,20},{20,24},{24,28},{28,32},{32,36}... | collective-permute-start | bytes 46088 | tf_op jit(solution)/shard_map/ppermute | solution.py:29
  416.3 21.6 %all-to-all-start.5 = ((bf16[4,384,512]{2,1,0:T(8,128)(2,1)}), bf16[4,384,512]{2,1,0:T(8,128)(2,1)S(1)}, u32[]{:S(2)}, u32[]{:S(2)}) async-start(bf16[4,384,512]{2,1,0:T(8,128)(2,1)} %bitcast.134), calls=%async_computation.5 | async-start | bytes 3145728 | tf_op jit(solution)/shard_map/all_to_all | solution.py:58
